TPU v7x, 32 devices: a whole 2x2x4 slice. The times are simulated.
32 devices in a mesh: sp: 16 (over z, y, x), tp: 2 (over core).
Axes of the slice: x: 2, y: 2, z: 4, core: 2. Of those that a mesh axis runs over, the one named last changes fastest.
Arguments:
- mixer_in: bfloat16 [8192, 1024], P('sp', 'tp'), may hold values from -6 to 6
- residual: bfloat16 [8192, 2048], P(('sp', 'tp')), may hold values from -6 to 6
- decay_real: float32 [64, 64], P('tp'), may hold values from -2 to 0, as said below
- decay_imag: float32 [64, 64], P('tp'), may hold values from 1 to 200
- log_step: float32 [64], P('tp'), may hold values from -3.9 to -2.5
- in_real: float32 [64, 64, 16], P('tp'), may hold values from -1 to 1
- in_imag: float32 [64, 64, 16], P('tp'), may hold values from -1 to 1
- output_real: float32 [64, 16, 64], P('tp'), may hold values from -0.5 to 0.5
- output_imaginary: float32 [64, 16, 64], P('tp'), may hold values from -0.5 to 0.5
- skip: float32 [1024], P('tp'), may hold values from -4 to 4
- out_proj: bfloat16 [1024, 2048], P('tp'), may hold values from -0.1875 to 0.1875
- norm_gain: float32 [2048], replicated, may hold values from 0.1 to 1.9
- w_gate: bfloat16 [2048, 5632], P('sp', 'tp'), may hold values from -0.125 to 0.125
- w_up: bfloat16 [2048, 5632], P('sp', 'tp'), may hold values from -0.125 to 0.125
- w_down: bfloat16 [5632, 2048], P('tp', 'sp'), may hold values from -0.078125 to 0.078125
Outputs:
- output: bfloat16 [8192, 2048], P(('sp', 'tp'))
Inputs may be any that keep to these rules, and one draw needn't show every extreme that they name: `decay_real`: every entry is negative.
All inputs are finite; a program needn't handle non-finite values.
Results may differ from a plain program's by a relative error of at most 0.02.
Values may be sent and summed in bfloat16 or wider, within the bound.
A program may use at most 128 MiB of HBM per device.

v0:
```python
import jax
import jax.numpy as jnp
from jax import lax
from jax.sharding import PartitionSpec as P


def prefix(value, axis, join, neutral):
    count, mine = (lax.axis_size(axis), lax.axis_index(axis))
    pieces = jax.tree.map(lambda part: lax.all_gather(part, axis), value)
    subtotal = jax.tree.map(
        lambda part, zero: jnp.full_like(part, 0) + jnp.asarray(zero, part.dtype), value, neutral
    )

    def step(position, subtotal):
        longer = join(subtotal, jax.tree.map(lambda part: part[position], pieces))
        return jax.tree.map(lambda new, old: jnp.where(position < mine, new, old), longer, subtotal)

    return lax.fori_loop(0, count - 1, step, subtotal)


def discrete(decay_real, decay_imag, log_step, in_real, in_imag):
    step_size = jnp.exp(log_step)[:, None]
    magnitude = jnp.exp(decay_real * step_size)
    angle = decay_imag * step_size
    power_re = magnitude * jnp.cos(angle)
    power_im = magnitude * jnp.sin(angle)
    denom = decay_real * decay_real + decay_imag * decay_imag
    ratio_re = ((power_re - 1.0) * decay_real + power_im * decay_imag) / denom
    ratio_im = (power_im * decay_real - (power_re - 1.0) * decay_imag) / denom
    drive_re = ratio_re[..., None] * in_real - ratio_im[..., None] * in_imag
    drive_im = ratio_re[..., None] * in_imag + ratio_im[..., None] * in_real
    return (power_re, power_im, drive_re, drive_im)


def combine(earlier, later):
    ar1, ai1, br1, bi1 = earlier
    ar2, ai2, br2, bi2 = later
    return (
        ar2 * ar1 - ai2 * ai1,
        ar2 * ai1 + ai2 * ar1,
        ar2 * br1 - ai2 * bi1 + br2,
        ar2 * bi1 + ai2 * br1 + bi2,
    )


def spread_blocks(matrix):
    groups = matrix.shape[0]
    unit_blocks = jnp.eye(groups, dtype=jnp.float32)[:, None, :, None]
    turned = jnp.transpose(matrix, (0, 2, 1))[:, :, None, :]
    return (unit_blocks * turned).reshape(groups * matrix.shape[2], groups * matrix.shape[1])


def local_states(power_re, power_im, drive_re, drive_im):
    rows, flat_size = drive_re.shape
    span = 8
    blocks = rows // span
    dr = drive_re.reshape(blocks, span, flat_size)
    di = drive_im.reshape(blocks, span, flat_size)
    cur_re = dr[:, 0]
    cur_im = di[:, 0]
    inner_re = [cur_re]
    inner_im = [cur_im]
    lift_re = [power_re]
    lift_im = [power_im]
    for index in range(1, span):
        cur_re, cur_im = (
            power_re * cur_re - power_im * cur_im + dr[:, index],
            power_re * cur_im + power_im * cur_re + di[:, index],
        )
        inner_re.append(cur_re)
        inner_im.append(cur_im)
        prev_re, prev_im = (lift_re[-1], lift_im[-1])
        lift_re.append(power_re * prev_re - power_im * prev_im)
        lift_im.append(power_re * prev_im + power_im * prev_re)
    inner_re = jnp.stack(inner_re, axis=1)
    inner_im = jnp.stack(inner_im, axis=1)
    lift_re = jnp.concatenate(lift_re, axis=0)[None]
    lift_im = jnp.concatenate(lift_im, axis=0)[None]
    block_re = jnp.broadcast_to(lift_re[0, span - 1][None], (blocks, flat_size))
    block_im = jnp.broadcast_to(lift_im[0, span - 1][None], (blocks, flat_size))
    totals = (block_re, block_im, cur_re, cur_im)
    distance = 1
    while distance < blocks:
        ones = jnp.ones((distance, flat_size), jnp.float32)
        zeros = jnp.zeros((distance, flat_size), jnp.float32)
        moved = (
            jnp.concatenate([ones, totals[0][:-distance]], axis=0),
            jnp.concatenate([zeros, totals[1][:-distance]], axis=0),
            jnp.concatenate([zeros, totals[2][:-distance]], axis=0),
            jnp.concatenate([zeros, totals[3][:-distance]], axis=0),
        )
        totals = combine(moved, totals)
        distance = distance * 2
    one_row = jnp.ones((1, flat_size), jnp.float32)
    zero_row = jnp.zeros((1, flat_size), jnp.float32)
    before_a_re = jnp.concatenate([one_row, totals[0][:-1]], axis=0)[:, None]
    before_a_im = jnp.concatenate([zero_row, totals[1][:-1]], axis=0)[:, None]
    before_re = jnp.concatenate([zero_row, totals[2][:-1]], axis=0)[:, None]
    before_im = jnp.concatenate([zero_row, totals[3][:-1]], axis=0)[:, None]
    state_real = inner_re + lift_re * before_re - lift_im * before_im
    state_imaginary = inner_im + lift_re * before_im + lift_im * before_re
    pw_re = lift_re * before_a_re - lift_im * before_a_im
    pw_im = lift_re * before_a_im + lift_im * before_a_re
    summary = (totals[0][-1], totals[1][-1], totals[2][-1], totals[3][-1])
    return (
        pw_re.reshape(rows, flat_size),
        pw_im.reshape(rows, flat_size),
        state_real.reshape(rows, flat_size),
        state_imaginary.reshape(rows, flat_size),
        summary,
    )


def on_device(
    mixer_in,
    residual,
    decay_real,
    decay_imag,
    log_step,
    in_real,
    in_imag,
    output_real,
    output_imaginary,
    skip,
    out_proj,
    norm_gain,
    w_gate,
    w_up,
    w_down,
):
    highest_precision = lax.Precision.HIGHEST
    power_re, power_im, bar_re, bar_im = discrete(
        decay_real, decay_imag, log_step, in_real, in_imag
    )
    flat_size = decay_real.shape[0] * decay_real.shape[1]
    read_in = jnp.concatenate([spread_blocks(bar_re), spread_blocks(bar_im)], axis=1)
    signal = mixer_in.astype(jnp.float32)
    drive = jnp.dot(signal, read_in, precision=highest_precision)
    drive_re = drive[:, :flat_size]
    drive_im = drive[:, flat_size:]
    pw_re, pw_im, state_real, state_imaginary, summary = local_states(
        power_re.reshape(1, flat_size), power_im.reshape(1, flat_size), drive_re, drive_im
    )
    zero_line = jnp.zeros((flat_size,), jnp.float32)
    identity = (jnp.ones((flat_size,), jnp.float32), zero_line, zero_line, zero_line)
    _, _, hold_re, hold_im = prefix(summary, "sp", combine, identity)
    state_real = state_real + pw_re * hold_re[None] - pw_im * hold_im[None]
    state_imaginary = state_imaginary + pw_re * hold_im[None] + pw_im * hold_re[None]
    read_out = jnp.concatenate(
        [spread_blocks(output_real), -spread_blocks(output_imaginary)], axis=0
    )
    mixed_before_norm = jnp.dot(
        jnp.concatenate([state_real, state_imaginary], axis=1),
        read_out,
        precision=highest_precision,
    )
    mixed_before_norm = mixed_before_norm + skip[None] * signal
    activated = jax.nn.gelu(mixed_before_norm).astype(jnp.bfloat16)
    partial_value = jnp.dot(activated, out_proj, preferred_element_type=jnp.float32).astype(
        jnp.bfloat16
    )
    mixed = lax.psum_scatter(
        lax.optimization_barrier(partial_value).astype(jnp.float32).astype(jnp.bfloat16),
        "tp",
        scatter_dimension=0,
        tiled=True,
    )
    carried = residual.astype(jnp.float32) + mixed.astype(jnp.float32)
    scale = lax.rsqrt(jnp.mean(carried * carried, axis=-1, keepdims=True) + 1e-06)
    normed = (carried * scale * norm_gain).astype(jnp.bfloat16)
    full_rows = lax.all_gather(normed, "tp", axis=0, tiled=True)
    gate = jnp.dot(
        full_rows,
        lax.all_gather(w_gate, "sp", axis=0, tiled=True),
        preferred_element_type=jnp.float32,
    )
    up = jnp.dot(
        full_rows,
        lax.all_gather(w_up, "sp", axis=0, tiled=True),
        preferred_element_type=jnp.float32,
    )
    down_columns = lax.all_gather(w_down, "sp", axis=1, tiled=True)
    hidden = (jax.nn.silu(gate) * up).astype(jnp.bfloat16)
    partial_value = jnp.dot(hidden, down_columns, preferred_element_type=jnp.float32).astype(
        jnp.bfloat16
    )
    down = lax.psum_scatter(
        lax.optimization_barrier(partial_value).astype(jnp.float32).astype(jnp.bfloat16),
        "tp",
        scatter_dimension=0,
        tiled=True,
    )
    return (carried + 0.5 * down.astype(jnp.float32)).astype(jnp.bfloat16)


def solution(mesh):
    return jax.shard_map(
        on_device,
        mesh=mesh,
        in_specs=(
            P("sp", "tp"),
            P(("sp", "tp"), None),
            P("tp", None),
            P("tp", None),
            P("tp"),
            P("tp", None, None),
            P("tp", None, None),
            P("tp", None, None),
            P("tp", None, None),
            P("tp"),
            P("tp", None),
            P(),
            P("sp", "tp"),
            P("sp", "tp"),
            P("tp", "sp"),
        ),
        out_specs=P(("sp", "tp"), None),
        check_vma=False,
    )
```

profile of v0, /device:TPU:0, one launch (start us, length us, event | category | flops | bytes accessed | tf_op | source)
XLA Modules:
  0.0 897.7 jit_solution(369592521946466958)
XLA Ops:
  9.7 8.3 broadcast_multiply_fusion.2
  18.1 7.8 mul.1865
  25.9 7.9 mul.1870
  33.8 10.5 %fusion.11 = f32[512,4096]{1,0:T(8,128)S(1)} fusion(bf16[512,512]{1,0:T(8,128)(2,1)S(1)} %copy-done.39, f32[512,2048]{1,0:T(8,128)} %mul.1870, f32[512,2048]{1,0:T(8,128)} %mul.1865), kind=kOutput, calls=%fused_computation.18 | convolution fusion | flops 12886999040 | bytes 17301504 | tf_op jit(solution)/shard_map/dot_general | solution.py:138
  47.9 2.7 fusion.62
  50.6 3.0 bitcast_add_fusion.9
  53.6 5.1 multiply_subtract_fusion.3
  61.5 6.1 copy_add_fusion.1
  76.0 2.5 copy.103
  89.2 43.1 %all-gather.2 = f32[16,1,2048]{2,1,0:T(1,128)S(1)} all-gather(f32[1,1,2048]{2,1,0:T(1,128)S(1)} %slice_bitcast_fusion.3), channel_id=1, replica_groups=mesh['sp'=16,'tp'=2] {'sp'}, dimensions={0}, use_global_device_ids=true | all-gather | bytes 139264 | tf_op jit(solution)/shard_map/all_gather | solution.py:9
  132.3 36.1 %all-gather.1 = f32[16,1,2048]{2,1,0:T(1,128)S(1)} all-gather(f32[1,1,2048]{2,1,0:T(1,128)S(1)} %slice_bitcast_fusion.4), channel_id=1, replica_groups=mesh['sp'=16,'tp'=2] {'sp'}, dimensions={0}, use_global_device_ids=true | all-gather | bytes 139264 | tf_op jit(solution)/shard_map/all_gather | solution.py:9
  168.5 38.2 %all-gather = f32[16,1,2048]{2,1,0:T(1,128)S(1)} all-gather(f32[1,1,2048]{2,1,0:T(1,128)S(1)} %slice_bitcast_fusion.5), channel_id=1, replica_groups=mesh['sp'=16,'tp'=2] {'sp'}, dimensions={0}, use_global_device_ids=true | all-gather | bytes 139264 | tf_op jit(solution)/shard_map/all_gather | solution.py:9
  207.5 36.2 %all-gather.3 = f32[16,1,2048]{2,1,0:T(1,128)S(1)} all-gather(f32[1,1,2048]{2,1,0:T(1,128)S(1)} %slice_bitcast_fusion.2), channel_id=1, replica_groups=mesh['sp'=16,'tp'=2] {'sp'}, dimensions={0}, use_global_device_ids=true | all-gather | bytes 139264 | tf_op jit(solution)/shard_map/all_gather | solution.py:9
  244.3 26.6 %while.16 = (s32[]{:T(128)}, f32[2048]{0:T(1024)S(1)}, f32[2048]{0:T(1024)S(1)}, s32[]{:T(128)}, f32[16,2048]{1,0:T(8,128)}, /*index=5*/f32[16,2048]{1,0:T(8,128...) while((s32[]{:T(128)}, f32[2048]{0:T(1024)S(1)}, f32[2048]{0:T(1024)S(1)}, ...), condition=%wide.region_1.2_spmd.clone, body=%wide.region_0.1_spmd.clone.sunk | while | flops 24580 | bytes 131201 | solution.py:18
  284.8 8.1 broadcast_multiply_fusion
  293.0 7.8 mul.2031
  300.8 7.8 neg.11
  310.5 11.9 %stack.5 = f32[64,8,2048]{2,1,0:T(8,128)} concatenate(f32[64,1,2048]{2,1,0:T(1,128)S(1)} %get-tuple-element.246, f32[64,1,2048]{2,1,0:T(1,128)} %copy.106, f32[64,1,2048]{2,1,0:T(1,128)} %copy.107, f32[64,1,2048]{2,1,0:T(1,128)} %copy.108, f32[64,1,2048]{2,1,0:T(1,128)} %copy.109, f32[64,1,2048]{2,1,0:T(1,128)} %copy.110, f32[64,1,2048]{2,1,0:T(1,128)} %copy.111, ...), dimensions={1} | concatenate | bytes 8388608 | tf_op jit(solution)/shard_map/stack | solution.py:76
  322.4 12.0 %stack.4 = f32[64,8,2048]{2,1,0:T(8,128)} concatenate(f32[64,1,2048]{2,1,0:T(1,128)S(1)} %get-tuple-element.248, f32[64,1,2048]{2,1,0:T(1,128)} %copy.98, f32[64,1,2048]{2,1,0:T(1,128)} %copy.99, f32[64,1,2048]{2,1,0:T(1,128)} %copy.100, f32[64,1,2048]{2,1,0:T(1,128)} %copy.101, f32[64,1,2048]{2,1,0:T(1,128)} %copy.102, f32[64,1,2048]{2,1,0:T(1,128)} %copy.103, ...), dimensions={1} | concatenate | bytes 8388608 | tf_op jit(solution)/shard_map/stack | solution.py:75
  334.4 7.0 fusion.15
  342.3 16.5 %fusion.24 = bf16[512,512]{1,0:T(8,128)(2,1)S(1)} fusion(bf16[512,512]{1,0:T(8,128)(2,1)S(1)} %copy-done.40, f32[2048,512]{0,1:T(8,128)S(1)} %copy-done.22, f32[2048,512]{0,1:T(8,128)S(1)} %copy-done.21, f32[512,2048]{1,0:T(8,128)} %get-tuple-element.258, f32[512,2048]{1,0:T(8,128)S(1)} %get-tuple-element.257, f32[512]{0:T(512)S(1)} %copy-done.50), kind=kOutput, calls=%fused_computation.49 | convolution fusion | flops 12892241920 | bytes 17827840 | tf_op jit(solution)/shard_map/dot_general | solution.py:152
  358.8 2.6 convolution_convert_fusion.1
  361.5 7.6 reduce-scatter.3.cloned.1.call-done
  370.8 2.6 multiply_convert_fusion.1
  375.3 10.1 %all-gather.9.cloned.1.call-done = bf16[512,2048]{1,0:T(8,128)(2,1)} async-done(((bf16[256,2048]{1,0:T(8,128)(2,1)}), bf16[512,2048]{1,0:T(8,128)(2,1)}) %all-gather.9.cloned.1.call-update) | async-done | bytes 2097168 | tf_op jit(solution)/shard_map/all_gather | solution.py:171
  385.4 145.4 %all-gather.11.cloned.1.call-done = bf16[2048,2816]{1,0:T(8,128)(2,1)} async-done(((bf16[128,2816]{1,0:T(8,128)(2,1)}), bf16[2048,2816]{1,0:T(8,128)(2,1)}) %all-gather.11.cloned.1.call-update) | async-done | bytes 11534352 | tf_op jit(solution)/shard_map/all_gather | solution.py:174
  530.8 12.7 %fusion.63 = f32[512,2816]{1,0:T(8,128)} fusion(bf16[512,2048]{1,0:T(8,128)(2,1)} %all-gather.9.cloned.1.call-done, bf16[2048,2816]{1,0:T(8,128)(2,1)} %all-gather.11.cloned.1.call-done), kind=kOutput, calls=%fused_computation.183 | convolution fusion | flops 5905580032 | bytes 19398656 | tf_op jit(solution)/shard_map/dot_general | solution.py:172
  543.5 129.6 %all-gather.13.cloned.1.call-done = bf16[2048,2816]{1,0:T(8,128)(2,1)} async-done(((bf16[128,2816]{1,0:T(8,128)(2,1)}), bf16[2048,2816]{1,0:T(8,128)(2,1)}) %all-gather.13.cloned.1.call-update) | async-done | bytes 11534352 | tf_op jit(solution)/shard_map/all_gather | solution.py:179
  673.0 182.8 %all-gather.15.cloned.1.call-done = bf16[2816,2048]{1,0:T(8,128)(2,1)} async-done(((bf16[2816,128]{1,0:T(8,128)(2,1)}), bf16[2816,2048]{1,0:T(8,128)(2,1)}) %all-gather.15.cloned.1.call-update) | async-done | bytes 11534352 | tf_op jit(solution)/shard_map/all_gather | solution.py:182
  855.8 23.4 %convolution_convert_fusion = bf16[512,2048]{1,0:T(8,128)(2,1)} fusion(bf16[2816,2048]{1,0:T(8,128)(2,1)} %all-gather.15.cloned.1.call-done, f32[512,2816]{1,0:T(8,128)} %fusion.63, bf16[512,2048]{1,0:T(8,128)(2,1)} %all-gather.9.cloned.1.call-done, bf16[2048,2816]{1,0:T(8,128)(2,1)} %all-gather.13.cloned.1.call-done), kind=kOutput, calls=%fused_computation.35 | convolution fusion | flops 11820859392 | bytes 33030144 | tf_op jit(solution)/shard_map/dot_general | solution.py:184
  879.2 8.1 reduce-scatter.5.cloned.1.call-done
  887.3 3.1 add_convert_fusion
  (232 shorter events, 75.8 us)
Async XLA Ops:
  6.5 352.3 %copy-start = (bf16[512,2048]{1,0:T(8,128)(2,1)S(1)}, bf16[512,2048]{1,0:T(8,128)(2,1)}, u32[]{:S(2)}) copy-start(bf16[512,2048]{1,0:T(8,128)(2,1)} %param.27) | copy-start | bytes 6291460
  6.5 362.6 %reduce-scatter.3.cloned.1.call-start = ((), (), s32[]{:S(2)}) async-start(), calls=%async_computation.2 | async-start | bytes 3145728 | tf_op jit(solution)/shard_map/reduce_scatter | solution.py:162
  6.5 11.5 %copy-start.47 = (f32[32,32]{0,1:T(8,128)}, f32[32,32]{0,1:T(8,128)S(1)}, u32[]{:S(2)}) copy-start(f32[32,32]{0,1:T(8,128)S(1)} %fusion.52) | copy-start | bytes 12292
  61.2 8.2 copy-start.41
  76.0 9.8 %copy-start.36 = (f32[64,1,2048]{2,0,1:T(8,128)S(1)}, f32[64,1,2048]{2,0,1:T(8,128)}, u32[]{:S(2)}) copy-start(f32[64,1,2048]{2,0,1:T(8,128)} %get-tuple-element.196) | copy-start | bytes 1572868
  76.0 11.2 %copy-start.35 = (f32[64,1,2048]{2,0,1:T(8,128)S(1)}, f32[64,1,2048]{2,0,1:T(8,128)}, u32[]{:S(2)}) copy-start(f32[64,1,2048]{2,0,1:T(8,128)} %get-tuple-element.194) | copy-start | bytes 1572868
  76.0 12.5 %copy-start.24 = (f32[64,2048]{1,0:T(8,128)S(1)}, f32[64,2048]{1,0:T(8,128)}, u32[]{:S(2)}) copy-start(f32[64,2048]{1,0:T(8,128)} %fusion.38) | copy-start | bytes 1572868
  76.0 12.5 %copy-start.23 = (f32[64,2048]{1,0:T(8,128)S(1)}, f32[64,2048]{1,0:T(8,128)}, u32[]{:S(2)}) copy-start(f32[64,2048]{1,0:T(8,128)} %get-tuple-element.206) | copy-start | bytes 1572868
  76.0 12.5 %copy-start.9 = (f32[64,2048]{1,0:T(8,128)S(1)}, f32[64,2048]{1,0:T(8,128)}, u32[]{:S(2)}) copy-start(f32[64,2048]{1,0:T(8,128)} %copy-done.8) | copy-start | bytes 1572868
  76.0 12.5 %copy-start.11 = (f32[64,2048]{1,0:T(8,128)S(1)}, f32[64,2048]{1,0:T(8,128)}, u32[]{:S(2)}) copy-start(f32[64,2048]{1,0:T(8,128)} %copy-done.10) | copy-start | bytes 1572868
  76.0 12.5 %copy-start.38 = (f32[48,2048]{1,0:T(8,128)S(1)}, f32[48,2048]{1,0:T(8,128)}, u32[]{:S(2)}) copy-start(f32[48,2048]{1,0:T(8,128)} %slice.234) | copy-start | bytes 1179652
  88.8 118.6 %copy-start.25 = (f32[64,2048]{1,0:T(8,128)}, f32[64,2048]{1,0:T(8,128)S(1)}, u32[]{:S(2)}) copy-start(f32[64,2048]{1,0:T(8,128)S(1)} %get-tuple-element.203) | copy-start | bytes 1572868
  89.1 118.3 %copy-start.26 = (f32[64,2048]{1,0:T(8,128)}, f32[64,2048]{1,0:T(8,128)S(1)}, u32[]{:S(2)}) copy-start(f32[64,2048]{1,0:T(8,128)S(1)} %get-tuple-element.262) | copy-start | bytes 1572868
  89.1 154.5 %copy-start.27 = (f32[64,2048]{1,0:T(8,128)}, f32[64,2048]{1,0:T(8,128)S(1)}, u32[]{:S(2)}) copy-start(f32[64,2048]{1,0:T(8,128)S(1)} %get-tuple-element.261) | copy-start | bytes 1572868
  89.1 154.5 %copy-start.28 = (f32[64,2048]{1,0:T(8,128)}, f32[64,2048]{1,0:T(8,128)S(1)}, u32[]{:S(2)}) copy-start(f32[64,2048]{1,0:T(8,128)S(1)} %get-tuple-element.267) | copy-start | bytes 1572868
  271.0 8.2 copy-start.34
  271.0 9.6 %copy-start.33 = (f32[64,1,2048]{2,0,1:T(8,128)S(1)}, f32[64,1,2048]{2,0,1:T(8,128)}, u32[]{:S(2)}) copy-start(f32[64,1,2048]{2,0,1:T(8,128)} %get-tuple-element.193) | copy-start | bytes 1572868
  271.0 11.0 %copy-start.32 = (f32[64,1,2048]{2,0,1:T(8,128)S(1)}, f32[64,1,2048]{2,0,1:T(8,128)}, u32[]{:S(2)}) copy-start(f32[64,1,2048]{2,0,1:T(8,128)} %get-tuple-element.201) | copy-start | bytes 1572868
  271.0 12.3 %copy-start.31 = (f32[64,1,2048]{2,0,1:T(8,128)S(1)}, f32[64,1,2048]{2,0,1:T(8,128)}, u32[]{:S(2)}) copy-start(f32[64,1,2048]{2,0,1:T(8,128)} %get-tuple-element.199) | copy-start | bytes 1572868
  271.0 13.6 %copy-start.45 = (f32[32,16,64]{2,1,0:T(8,128)S(1)}, f32[32,16,64]{2,1,0:T(8,128)}, u32[]{:S(2)}) copy-start(f32[32,16,64]{2,1,0:T(8,128)} %param.24) | copy-start | bytes 393220
  273.0 11.7 %copy-start.46 = (f32[32,16,64]{2,1,0:T(8,128)S(1)}, f32[32,16,64]{2,1,0:T(8,128)}, u32[]{:S(2)}) copy-start(f32[32,16,64]{2,1,0:T(8,128)} %param.25) | copy-start | bytes 393220
  273.0 11.8 %copy-start.48 = (f32[32,32]{0,1:T(8,128)S(1)}, f32[32,32]{0,1:T(8,128)}, u32[]{:S(2)}) copy-start(f32[32,32]{0,1:T(8,128)} %copy-done.47) | copy-start | bytes 12292
  322.4 12.0 %copy-start.37 = (f32[64,2048]{1,0:T(8,128)S(1)}, f32[64,2048]{1,0:T(8,128)}, u32[]{:S(2)}) copy-start(f32[64,2048]{1,0:T(8,128)} %concatenate.124) | copy-start | bytes 1572868
  322.4 12.0 %copy-start.42 = (f32[8,2048]{1,0:T(8,128)S(1)}, f32[8,2048]{1,0:T(8,128)}, u32[]{:S(2)}) copy-start(f32[8,2048]{1,0:T(8,128)} %copy-done.41) | copy-start | bytes 196612
  322.4 12.0 %copy-start.44 = (f32[8,2048]{1,0:T(8,128)S(1)}, f32[8,2048]{1,0:T(8,128)}, u32[]{:S(2)}) copy-start(f32[8,2048]{1,0:T(8,128)} %copy-done.43) | copy-start | bytes 196612
  358.8 10.3 %copy-start.3 = (bf16[256,2048]{1,0:T(8,128)(2,1)S(1)}, bf16[256,2048]{1,0:T(8,128)(2,1)}, u32[]{:S(2)}) copy-start(bf16[256,2048]{1,0:T(8,128)(2,1)} %param.18) | copy-start | bytes 3145732
  361.4 9.3 %copy-start.49 = (f32[2048]{0:T(1024)S(1)}, f32[2048]{0:T(1024)}, u32[]{:S(2)}) copy-start(f32[2048]{0:T(1024)} %param.28) | copy-start | bytes 24580
  361.4 23.9 %all-gather.9.cloned.1.call-start = ((), (), s32[]{:S(2)}) async-start(), calls=%async_computation.3 | async-start | bytes 3145728 | tf_op jit(solution)/shard_map/all_gather | solution.py:171
  373.4 157.4 %all-gather.11.cloned.1.call-start = ((), (), s32[]{:S(2)}) async-start(), calls=%async_computation.4 | async-start | bytes 12255232 | tf_op jit(solution)/shard_map/all_gather | solution.py:174
  374.1 298.9 %all-gather.13.cloned.1.call-start = ((), (), s32[]{:S(2)}) async-start(), calls=%async_computation.5 | async-start | bytes 12255232 | tf_op jit(solution)/shard_map/all_gather | solution.py:179
  374.7 481.1 %all-gather.15.cloned.1.call-start = ((), (), s32[]{:S(2)}) async-start(), calls=%async_computation.6 | async-start | bytes 12255232 | tf_op jit(solution)/shard_map/all_gather | solution.py:182
  375.3 512.1 %reduce-scatter.5.cloned.1.call-start = ((), (), s32[]{:S(2)}) async-start(), calls=%async_computation.7 | async-start | bytes 3145728 | tf_op jit(solution)/shard_map/reduce_scatter | solution.py:187
  (25 other events, 152.3 us)
Sparse Core Ops, SparseCore 0:
  361.6 7.4 reduce-scatter.2
  373.5 11.8 all-gather.8
  388.1 142.5 all-gather.10
  533.4 139.5 all-gather.12
  675.6 180.2 all-gather.14
  879.3 7.9 reduce-scatter.4
where the time goes:
time: 910 us; the launch traced here: 898 us
  waiting for transfers between devices  485 us (53%)
  blocking collectives  154 us (17%)
  local copies, waits for them, and re-layouts  123 us (14%)
  matrix products  65.6 us (7%)
  other arithmetic  54.9 us (6%)
  between operations  14.7 us (2%)
    all_gather x1, waiting for transfers between devices, on_device(): down_columns = lax.all_gather(w_down, 'sp', axis=1, tiled=True)  183 us
    all_gather x4, blocking collectives, prefix(): pieces = jax.tree.map(lambda part: lax.all_gather(part, axis), value)  154 us
    all_gather x1, waiting for transfers between devices, on_device(): lax.all_gather(w_gate, 'sp', axis=0, tiled=True)  145 us
    all_gather x1, waiting for transfers between devices, on_device(): lax.all_gather(w_up, 'sp', axis=0, tiled=True)  130 us
    dynamic_slice x30, local copies, waits for them, and re-layouts, step(): longer = join(subtotal, jax.tree.map(lambda part: part[position], pieces))  25.8 us
    mul x3, local copies, waits for them, and re-layouts, spread_blocks(): unit_blocks * turned  23.5 us
    dot_general x1, matrix products, on_device(): jnp.dot(hidden, down_columns, preferred_element_type=jnp.float32)  23.4 us
  transfers between devices with their start and end apart: 6, of which 6 were waited for; matrix products, arithmetic and copies ran while one was open for 1% of the time, Pallas kernels for 0%

commit v1 on v0

v1 whole, which is shorter than its diff:
```python
import functools

import jax
import jax.numpy as jnp
from jax import lax
from jax.experimental import pallas as pl
from jax.experimental.pallas import tpu as pltpu
from jax.sharding import Mesh
from jax.sharding import PartitionSpec as P

F32 = jnp.float32
BF16 = jnp.bfloat16
SP = ("h", "u", "m", "v")
PEERS = ("u", "v")
GATHER = 8
CHUNKS = 8
MESH = pl.DeviceIdType.MESH


def discrete(decay_real, decay_imag, log_step, in_real, in_imag):
    step_size = jnp.exp(log_step)[:, None]
    magnitude = jnp.exp(decay_real * step_size)
    angle = decay_imag * step_size
    power_re = magnitude * jnp.cos(angle)
    power_im = magnitude * jnp.sin(angle)
    denom = decay_real * decay_real + decay_imag * decay_imag
    ratio_re = ((power_re - 1.0) * decay_real + power_im * decay_imag) / denom
    ratio_im = (power_im * decay_real - (power_re - 1.0) * decay_imag) / denom
    drive_re = ratio_re[..., None] * in_real - ratio_im[..., None] * in_imag
    drive_im = ratio_re[..., None] * in_imag + ratio_im[..., None] * in_real
    return (power_re, power_im, drive_re, drive_im)


def cmul(ar, ai, br, bi):
    return ar * br - ai * bi, ar * bi + ai * br


def cpow(ar, ai, count):
    result = None
    while count:
        if count & 1:
            result = (ar, ai) if result is None else cmul(*result, ar, ai)
        count >>= 1
        if count:
            ar, ai = cmul(ar, ai, ar, ai)
    return result


def iota(shape, dim):
    return lax.broadcasted_iota(jnp.int32, shape, dim)


def tiled(block, copies, across, down):
    rows, columns = block.shape
    wide = (columns, columns * copies)
    pick = (iota(wide, 0) == lax.rem(iota(wide, 1), columns)).astype(BF16)
    full = jnp.dot(block, pick, preferred_element_type=F32)
    keep = lax.div(iota(full.shape, 0), down) == lax.div(iota(full.shape, 1), across)
    return jnp.where(keep, full, 0.0).astype(BF16)


def front(sizes, x_ref, b_ref, c_ref, a_ref, k_ref, wo_ref, res_ref, gain_ref, *rest):
    quarters, rest = rest[:3], rest[3:]
    weights, (rows_ref, carried_ref), rest = rest[:3], rest[3:5], rest[5:]
    (work, read_in, read_out, ends, total, gathered, act, share, others,
     send_sem, recv_sem, local_sem) = rest
    blocks, rows, cb = x_ref.shape
    sb = a_ref.shape[2]
    depth = quarters[0].shape[2]
    width = wo_ref.shape[1]
    span = rows // CHUNKS
    nh, nm, tp = sizes["h"], sizes["m"], sizes["tp"]
    n = nh * 4 * nm
    h, u, m, v, core = (lax.axis_index(name) for name in (*SP, "tp"))
    index = lambda h, u, m, v: ((h * 2 + u) * nm + m) * 2 + v
    me = index(h, u, m, v)
    peer = lambda k: (1 - u if k & 2 else u, 1 - v if k & 1 else v)
    counter = iter(range(send_sem.shape[0]))

    def send(src, dst, device):
        slot = next(counter)
        copy = pltpu.make_async_remote_copy(
            src_ref=src, dst_ref=dst, send_sem=send_sem.at[slot], recv_sem=recv_sem.at[slot],
            device_id=device, device_id_type=MESH,
        )
        copy.start()
        return copy

    def place(ref, position):
        if depth % 128:
            return ref.at[position]
        return ref.at[:, pl.ds(pl.multiple_of(position * depth, depth), depth)]

    barrier = pltpu.get_barrier_semaphore()
    others_sp = []
    for k in range(1, n):
        to = lax.rem(me + k, n)
        there = (lax.div(to, 4 * nm), lax.rem(lax.div(to, 2 * nm), 2),
                 lax.rem(lax.div(to, 2), nm), lax.rem(to, 2), core)
        others_sp.append(there)
        pl.semaphore_signal(barrier, inc=1, device_id=there, device_id_type=MESH)
    for t in range(1, tp):
        pl.semaphore_signal(
            barrier, inc=1, device_id=(h, u, m, v, lax.rem(core + t, tp)), device_id_type=MESH
        )
    pl.semaphore_wait(barrier, n - 1 + tp - 1)

    sent = []
    first = {}
    over_h = {}
    over_m = {}

    def spread_h(w, k, src, position):
        for r in range(1, nh):
            pu, pv = peer(k)
            copy = send(src, place(weights[w], position), (lax.rem(h + r, nh), u, m, v, core))
            over_h[w, k, r] = copy

    def spread_m(w, k, r, src, position):
        for s in range(1, nm):
            over_m[w, k, r, s] = send(
                src, place(weights[w], position), (h, u, lax.rem(m + s, nm), v, core)
            )

    own = u * 2 + v
    for w in range(3):
        for k in (3, 1, 2):
            pu, pv = peer(k)
            first[w, k] = send(
                quarters[w].at[pu * 2 + pv], place(weights[w], me), (h, pu, m, pv, core)
            )
    locals_ = []
    for w in range(3):
        spread_h(w, 0, quarters[w].at[own], me)
        spread_m(w, 0, 0, quarters[w].at[own], me)
        copy = pltpu.make_async_copy(quarters[w].at[own], place(weights[w], me), local_sem.at[w])
        copy.start()
        locals_.append(copy)

    def scan(b, start, keep):
        work[...] = jnp.dot(x_ref[b], read_in[b], preferred_element_type=F32)
        br = jnp.broadcast_to(a_ref[b, 0:1, :], (CHUNKS, sb))
        bi = jnp.broadcast_to(a_ref[b, 1:2, :], (CHUNKS, sb))

        def step(i, state):
            at = pl.ds(pl.multiple_of(i * CHUNKS, CHUNKS), CHUNKS)
            nr, ni = cmul(br, bi, *state)
            nr, ni = nr + work[at, :sb], ni + work[at, sb:]
            if keep:
                work[at, :sb] = nr
                work[at, sb:] = ni
            return nr, ni

        return lax.fori_loop(0, span, step, start, unroll=8)

    @pl.loop(0, blocks)
    def _(b):
        states = b_ref.shape[3]
        for half in range(2):
            read_in[b, :, half * sb:(half + 1) * sb] = tiled(
                b_ref[b, half], GATHER, states, cb // GATHER
            )
            read_out[b, half * sb:(half + 1) * sb, :] = tiled(
                c_ref[b, half], GATHER, cb // GATHER, states
            )
        zero = jnp.zeros((CHUNKS, sb), F32)
        sr, si = scan(b, (zero, zero), False)
        ends[b, :, :sb] = sr
        ends[b, :, sb:] = si
        lr, li = cpow(a_ref[b, 0:1, :], a_ref[b, 1:2, :], span)
        er, ei = sr[0:1], si[0:1]
        for chunk in range(1, CHUNKS):
            er, ei = cmul(lr, li, er, ei)
            er, ei = er + sr[chunk:chunk + 1], ei + si[chunk:chunk + 1]
        total[b, :, :sb] = er
        total[b, :, sb:] = ei

    states_out = [send(total, gathered.at[me], there) for there in others_sp]
    gathered[me] = total[...]
    for copy in states_out:
        copy.wait_recv()

    @pl.loop(0, blocks)
    def _(b):
        lr, li = cpow(a_ref[b, 0:1, :], a_ref[b, 1:2, :], span)
        tr, ti = cpow(lr, li, CHUNKS)
        hr = jnp.zeros((1, sb), F32)
        hi = hr
        for device in range(n - 1):
            nr, ni = cmul(tr, ti, hr, hi)
            nr = nr + gathered[device, b, :, :sb]
            ni = ni + gathered[device, b, :, sb:]
            hr, hi = jnp.where(device < me, nr, hr), jnp.where(device < me, ni, hi)
        starts_r, starts_i = [hr], [hi]
        for chunk in range(CHUNKS - 1):
            nr, ni = cmul(lr, li, hr, hi)
            hr = nr + ends[b, chunk:chunk + 1, :sb]
            hi = ni + ends[b, chunk:chunk + 1, sb:]
            starts_r.append(hr)
            starts_i.append(hi)
        scan(b, (jnp.concatenate(starts_r, axis=0), jnp.concatenate(starts_i, axis=0)), True)
        mixed = jnp.dot(work[...].astype(BF16), read_out[b], preferred_element_type=F32)
        mixed = mixed + k_ref[b] * x_ref[b].astype(F32)
        mixed = jax.nn.gelu(mixed).astype(BF16)
        square = (rows, rows)
        source = lax.rem(iota(square, 0), span) * CHUNKS + lax.div(iota(square, 0), span)
        turn = (iota(square, 1) == source).astype(BF16)
        act[:, pl.ds(pl.multiple_of(b * cb, cb), cb)] = jnp.dot(
            turn, mixed, preferred_element_type=F32
        ).astype(BF16)

    keep_rows = rows // tp
    tile = min(512, width)
    mixed_copies = []
    for t in (*range(1, tp), 0):
        to = lax.rem(core + t, tp)

        @pl.loop(0, width // tile)
        def _(j):
            at = pl.ds(pl.multiple_of(j * tile, tile), tile)
            share[t, :, at] = jnp.dot(
                act[pl.ds(pl.multiple_of(to * keep_rows, keep_rows), keep_rows), :],
                wo_ref[:, at], preferred_element_type=F32,
            ).astype(BF16)

        if t:
            mixed_copies.append(send(share.at[t], others.at[t - 1], (h, u, m, v, to)))

    for w in range(3):
        for k in (1, 2, 3):
            first[w, k].wait_recv()
            pu, pv = peer(k)
            position = index(h, pu, m, pv)
            spread_h(w, k, place(weights[w], position), position)
            spread_m(w, k, 0, place(weights[w], position), position)

    for copy in mixed_copies:
        copy.wait_recv()
    line = min(32, keep_rows)

    @pl.loop(0, keep_rows // line)
    def _(i):
        at = pl.ds(pl.multiple_of(i * line, line), line)
        mixed = share[0, at, :].astype(F32)
        for t in range(1, tp):
            mixed = mixed + others[t - 1, at, :].astype(F32)
        carried = res_ref[at, :].astype(F32) + mixed.astype(BF16).astype(F32)
        scale = lax.rsqrt(jnp.mean(carried * carried, axis=-1, keepdims=True) + 1e-06)
        carried_ref[at, :] = carried
        rows_ref[0, 0, at, :] = (carried * scale * gain_ref[...]).astype(BF16)

    row_copies = {}
    for k in (3, 1, 2):
        pu, pv = peer(k)
        row_copies[k] = send(rows_ref.at[0, 0], rows_ref.at[0, k], (h, pu, m, pv, core))
    last = []
    for t in range(1, tp):
        last.append(send(rows_ref.at[0, 0], rows_ref.at[t, 0], (h, u, m, v, lax.rem(core + t, tp))))

    def pass_m(w, k):
        pu, pv = peer(k)
        for r in range(1, nh):
            over_h[w, k, r].wait_recv()
            position = index(lax.rem(h - r + nh, nh), pu, m, pv)
            spread_m(w, k, r, place(weights[w], position), position)

    for w in range(3):
        for k in range(4):
            pass_m(w, k)
        if w == 1:
            for k in (1, 2, 3):
                row_copies[k].wait_recv()
                for t in range(1, tp):
                    last.append(send(
                        rows_ref.at[0, k], rows_ref.at[t, k], (h, u, m, v, lax.rem(core + t, tp))
                    ))
    for copy in (*over_m.values(), *last):
        copy.wait_recv()
    for copy in (*first.values(), *over_h.values(), *over_m.values(), *states_out,
                 *mixed_copies, *row_copies.values(), *last):
        copy.wait_send()
    for copy in locals_:
        copy.wait()


def shift(value, axis, count, by):
    return lax.ppermute(value, axis, [(i, (i + by) % count) for i in range(count)])


def flip(value, axes, count, k):
    return lax.ppermute(value, axes, [(i, i ^ k) for i in range(count)])


def on_device(sizes, mixer_in, residual, decay_real, decay_imag, log_step, in_real, in_imag,
              output_real, output_imaginary, skip, out_proj, norm_gain, w_gate, w_up, w_down):
    tp, nh, nm = sizes["tp"], sizes["h"], sizes["m"]
    n = nh * 4 * nm
    rows, channels = mixer_in.shape
    keep_rows, width = residual.shape
    depth, hidden_units = w_gate.shape
    part = hidden_units // 4
    groups, states = decay_real.shape
    blocks = groups // GATHER
    cb, sb = channels // blocks, GATHER * states
    power_re, power_im, bar_re, bar_im = discrete(
        decay_real, decay_imag, log_step, in_real, in_imag
    )
    rows_first = lambda t: jnp.transpose(t, (0, 2, 1)).reshape(blocks, -1, t.shape[1])
    read_in = jnp.stack([rows_first(bar_re), rows_first(bar_im)], axis=1).astype(BF16)
    read_out = jnp.stack(
        [rows_first(output_real), -rows_first(output_imaginary)], axis=1
    ).astype(BF16)
    power = jnp.stack([power_re.reshape(blocks, sb), power_im.reshape(blocks, sb)], axis=1)
    x = mixer_in.reshape(CHUNKS, rows // CHUNKS, blocks, cb).transpose(2, 1, 0, 3)
    x = x.reshape(blocks, rows, cb)
    copies = 3 * (3 + 4 * (nh - 1) + 4 * nh * (nm - 1)) + (n - 1) + (tp - 1) + 3 + 4 * (tp - 1)
    laid = (part, n * depth) if depth % 128 == 0 else (n, part, depth)
    vmem = pl.BlockSpec(memory_space=pltpu.VMEM)
    full_gate, full_up, full_down, rows_all, carried = pl.pallas_call(
        functools.partial(front, sizes),
        in_specs=[vmem] * 11,
        out_specs=[vmem] * 5,
        out_shape=[jax.ShapeDtypeStruct(laid, BF16)] * 3 + [
            jax.ShapeDtypeStruct((tp, 4, keep_rows, width), BF16),
            jax.ShapeDtypeStruct((keep_rows, width), F32),
        ],
        scratch_shapes=[
            pltpu.VMEM((rows, 2 * sb), F32),
            pltpu.VMEM((blocks, cb, 2 * sb), BF16),
            pltpu.VMEM((blocks, 2 * sb, cb), BF16),
            pltpu.VMEM((blocks, CHUNKS, 2 * sb), F32),
            pltpu.VMEM((blocks, 1, 2 * sb), F32),
            pltpu.VMEM((n, blocks, 1, 2 * sb), F32),
            pltpu.VMEM((rows, channels), BF16),
            pltpu.VMEM((tp, keep_rows, width), BF16),
            pltpu.VMEM((tp - 1, keep_rows, width), BF16),
            pltpu.SemaphoreType.DMA((copies,)),
            pltpu.SemaphoreType.DMA((copies,)),
            pltpu.SemaphoreType.DMA((3,)),
        ],
        compiler_params=pltpu.CompilerParams(
            collective_id=0, has_side_effects=True, vmem_limit_bytes=60 * 2**20
        ),
        name="front",
    )(x, read_in, read_out, power, skip.reshape(blocks, 1, cb), out_proj, residual,
      norm_gain.reshape(1, width), w_gate.T.reshape(4, part, depth),
      w_up.T.reshape(4, part, depth), w_down.reshape(4, part, depth))
    if len(laid) == 3:
        full_gate, full_up, full_down = (
            t.transpose(1, 0, 2).reshape(part, width) for t in (full_gate, full_up, full_down)
        )

    flat = rows_all.reshape(-1, width)
    across = (((1,), (1,)), ((), ()))
    gate = lax.dot_general(flat, full_gate, across, preferred_element_type=F32)
    up = lax.dot_general(flat, full_up, across, preferred_element_type=F32)
    hidden = (jax.nn.silu(gate) * up).astype(BF16)
    down = jnp.dot(hidden, full_down, preferred_element_type=F32).astype(BF16)
    down = down.reshape(rows_all.shape)
    summed = down[0].astype(F32)
    for t in range(1, tp):
        summed = summed + shift(down[t], "tp", tp, -t).astype(F32)
    summed = summed.astype(BF16)
    total = summed[0].astype(F32)
    for k in range(1, 4):
        total = total + flip(summed[k], PEERS, 4, k).astype(F32)
    total = total.astype(BF16)
    return (carried + 0.5 * total.astype(F32)).astype(BF16)


def solution(mesh):
    sp, tp = mesh.shape["sp"], mesh.shape["tp"]
    sizes = {"h": sp // 8, "u": 2, "m": 2, "v": 2, "tp": tp}
    cut = Mesh(mesh.devices.reshape(tuple(sizes.values())), tuple(sizes))
    return jax.shard_map(
        functools.partial(on_device, sizes),
        mesh=cut,
        in_specs=(
            P(SP, "tp"),
            P((*SP, "tp"), None),
            P("tp", None),
            P("tp", None),
            P("tp"),
            P("tp", None, None),
            P("tp", None, None),
            P("tp", None, None),
            P("tp", None, None),
            P("tp"),
            P("tp", None),
            P(),
            P(SP, "tp"),
            P(SP, "tp"),
            P("tp", SP),
        ),
        out_specs=P((*SP, "tp"), None),
        check_vma=False,
    )
```

time: 910 us -> 277 us (0.30); the launches traced: 898 us -> 276 us
  waiting for transfers between devices: 485 us -> 52.7 us
  Pallas kernels: 0 us -> 166 us
  blocking collectives: 154 us -> 0 us
  local copies, waits for them, and re-layouts: 123 us -> 11.8 us
  other arithmetic: 54.9 us -> 11.6 us
  matrix products: 65.6 us -> 30.3 us
  between operations: 14.7 us -> 0.1 us
    all_gather x4 -> x0, waiting for transfers between devices: 468 us -> none  [the longest x1 183 us: on_device(): down_columns = lax.all_gather(w_down, 'sp', axis=1, tiled=True)]
    pallas_call x0 -> x1, Pallas kernels: none -> 166 us  [on_device(): pl.pallas_call(functools.partial(front, sizes), in_specs=[vmem] * 11, out...]
    all_gather x4 -> x0, blocking collectives: 154 us -> none  [prefix(): pieces = jax.tree.map(lambda part: lax.all_gather(part, axis), value)]
    ppermute x0 -> x4, waiting for transfers between devices: none -> 52.7 us  [the longest x3 45.6 us: flip(): return lax.ppermute(value, axes, [(i, i ^ k) for i in range(count)])]
    dot_general x5 -> x2, matrix products: 65.6 us -> 30.3 us  [the longest x1 19.1 us: on_device(): down = jnp.dot(hidden, full_down, preferred_element_type=F32).astype(BF16)]
    dynamic_slice x30 -> x0, local copies, waits for them, and re-layouts: 25.8 us -> none  [step(): longer = join(subtotal, jax.tree.map(lambda part: part[position], pieces))]
    mul x5 -> x0, local copies, waits for them, and re-layouts: 23.6 us -> none  [the longest x3 23.5 us: spread_blocks(): unit_blocks * turned]
    another operation x2 -> x3, local copies, waits for them, and re-layouts: 23.8 us -> 1.62 us  [the longest x2 1.34 us: on_device(): jnp.stack([power_re.reshape(blocks, sb), power_im.reshape(blocks, sb)], a...]
  transfers between devices with their start and end apart: 6 -> 4, of which waited for: 6 -> 3; matrix products, arithmetic and copies ran while one was open for 1% -> 0% of each run, Pallas kernels for 0% -> 0%
where the time goes in v1:
time: 277 us; the launch traced here: 276 us
  Pallas kernels  166 us (60%)
  waiting for transfers between devices  52.7 us (19%)
  matrix products  30.3 us (11%)
  local copies, waits for them, and re-layouts  11.8 us (4%)
  other arithmetic  11.6 us (4%)
  starting transfers between devices  3.62 us (1%)
    pallas_call x1, Pallas kernels, on_device(): pl.pallas_call(functools.partial(front, sizes), in_specs=[vmem] * 11, out...  166 us
    ppermute x3, waiting for transfers between devices, flip(): return lax.ppermute(value, axes, [(i, i ^ k) for i in range(count)])  45.6 us
    dot_general x1, matrix products, on_device(): down = jnp.dot(hidden, full_down, preferred_element_type=F32).astype(BF16)  19.1 us
    dot_general x1, matrix products, on_device(): gate = lax.dot_general(flat, full_gate, across, preferred_element_type=F32)  11.2 us
    ppermute x1, waiting for transfers between devices, shift(): lax.ppermute(value, axis, [(i, (i + by) % count) for i in range(count)])  7.15 us
  transfers between devices with their start and end apart: 4, of which 3 were waited for; matrix products, arithmetic and copies ran while one was open for 0% of the time, Pallas kernels for 0%

profile of v1, /device:TPU:0, one launch (start us, length us, event | category | flops | bytes accessed | tf_op | source)
XLA Modules:
  0.0 276.4 jit_solution(4454628951693175453)
XLA Ops:
  0.0 0.8 exp.10
  0.8 1.5 cosine_multiply_fusion
  2.3 0.7 stack_reshape.21
  3.0 0.7 stack_reshape.22
  3.6 1.0 convert_bitcast_fusion
  4.6 1.0 fusion.5
  5.6 0.3 copy.41
  5.9 0.3 copy.40
  6.2 1.2 reshape.49
  7.3 1.1 copy.45
  8.5 1.1 copy.38
  9.6 1.2 copy.39
  10.8 1.3 pad_maximum_fusion.2.a_ref
  12.1 0.0 copy-done.4
  12.1 0.8 subtract_convert_fusion
  12.9 0.7 pad_maximum_fusion.1.b_ref
  13.7 1.2 pad_maximum_fusion.c_ref
  14.9 166.3 %front.1 = (bf16[704,2048]{1,0:T(8,128)(2,1)}, bf16[704,2048]{1,0:T(8,128)(2,1)}, bf16[704,2048]{1,0:T(8,128)(2,1)}, bf16[2,4,256,2048]{3,2,1,0:T(8,128)(2,1)}, f32[256,2048]{1,0:T(8,128)}) custom-call(bf16[4,512,128]{2,1,0:T(8,128)(2,1)} %bitcast.48, bf16[4,2,128,64]{3,2,1,0:T(8,128)(2,1)} %pad_maximum_fusion.1.b_ref, ...), custom_call_target="tpu_custom_call" | custom-call | tf_op jit(solution)/shard_map/front/pallas_call | solution.py:319
  181.2 11.2 %fusion.9 = f32[2048,704]{0,1:T(8,128)} fusion(bf16[2048,2048]{1,0:T(8,128)(2,1)} %bitcast.58, bf16[704,2048]{1,0:T(8,128)(2,1)} %get-tuple-element.12), kind=kOutput, calls=%fused_computation.31 | convolution fusion | flops 5905580032 | bytes 17039360 | tf_op jit(solution)/shard_map/dot_general | solution.py:355
  192.5 19.1 %convolution_convert_fusion = bf16[2048,2048]{1,0:T(8,128)(2,1)} fusion(bf16[704,2048]{1,0:T(8,128)(2,1)} %get-tuple-element.14, f32[2048,704]{0,1:T(8,128)} %fusion.9, bf16[2048,2048]{1,0:T(8,128)(2,1)} %bitcast.59, bf16[704,2048]{1,0:T(8,128)(2,1)S(1)} %copy-done.5), kind=kOutput, calls=%fused_computation.2 | convolution fusion | flops 11824005120 | bytes 28311552 | tf_op jit(solution)/shard_map/dot_general | solution.py:358
  211.5 4.1 %fusion.8 = (bf16[1024,2048]{1,0:T(8,128)(2,1)S(1)}, bf16[1024,2048]{1,0:T(8,128)(2,1)S(1)}) fusion(bf16[2048,2048]{1,0:T(8,128)(2,1)} %convolution_convert_fusion), kind=kLoop, calls=%fused_computation.30 | loop fusion | bytes 16777216 | tf_op jit(solution)/shard_map/slice | solution.py:362
  215.6 0.1 collective-permute-start
  215.7 7.1 %collective-permute-done = bf16[4,256,2048]{2,1,0:T(8,128)(2,1)S(1)} collective-permute-done((bf16[4,256,2048]{2,1,0:T(8,128)(2,1)S(1)}, bf16[4,256,2048]{2,1,0:T(8,128)(2,1)S(1)}, u32[]{:S(2)}, u32[]{:S(2)}) %collective-permute-start) | collective-permute-done | bytes 4194336 | tf_op jit(solution)/shard_map/ppermute | solution.py:287
  222.9 2.3 fusion
  225.2 0.3 slice_bitcast_fusion.2
  225.5 1.6 collective-permute-start.1
  227.1 1.3 collective-permute-start.3
  228.5 0.6 collective-permute-start.2
  229.1 44.2 %collective-permute-done.1 = bf16[256,2048]{1,0:T(8,128)(2,1)S(1)} collective-permute-done((bf16[256,2048]{1,0:T(8,128)(2,1)S(1)}, bf16[256,2048]{1,0:T(8,128)(2,1)S(1)}, u32[]{:S(2)}, u32[]{:S(2)}) %collective-permute-start.1) | collective-permute-done | bytes 1048608 | tf_op jit(solution)/shard_map/ppermute | solution.py:291
  273.2 0.0 collective-permute-done.3
  273.2 1.4 collective-permute-done.2
  274.6 1.8 add_convert_fusion
  (11 shorter events, 0.0 us)
Async XLA Ops:
  0.0 8.5 %copy-start.1 = (bf16[128,2816]{1,0:T(8,128)(2,1)S(1)}, bf16[128,2816]{1,0:T(8,128)(2,1)}, u32[]{:S(2)}) copy-start(bf16[128,2816]{1,0:T(8,128)(2,1)} %param.27) | copy-start | bytes 2162692
  0.0 9.6 %copy-start.2 = (bf16[128,2816]{1,0:T(8,128)(2,1)S(1)}, bf16[128,2816]{1,0:T(8,128)(2,1)}, u32[]{:S(2)}) copy-start(bf16[128,2816]{1,0:T(8,128)(2,1)} %param.28) | copy-start | bytes 2162692
  0.0 12.1 %copy-start.3 = (f32[32,64,16]{1,2,0:T(8,128)S(1)}, f32[32,64,16]{1,2,0:T(8,128)}, u32[]{:S(2)}) copy-start(f32[32,64,16]{1,2,0:T(8,128)} %param.21) | copy-start | bytes 393220
  0.0 12.1 %copy-start.4 = (f32[32,64,16]{1,2,0:T(8,128)S(1)}, f32[32,64,16]{1,2,0:T(8,128)}, u32[]{:S(2)}) copy-start(f32[32,64,16]{1,2,0:T(8,128)} %param.20) | copy-start | bytes 393220
  181.2 11.3 %copy-start.5 = (bf16[704,2048]{1,0:T(8,128)(2,1)S(1)}, bf16[704,2048]{1,0:T(8,128)(2,1)}, u32[]{:S(2)}) copy-start(bf16[704,2048]{1,0:T(8,128)(2,1)} %get-tuple-element.13) | copy-start | bytes 8650756
  215.6 7.2 %collective-permute-start = (bf16[4,256,2048]{2,1,0:T(8,128)(2,1)S(1)}, bf16[4,256,2048]{2,1,0:T(8,128)(2,1)S(1)}, u32[]{:S(2)}, u32[]{:S(2)}) collective-permute-start(bf16[4,256,2048]{2,1,0:T(8,128)(2,1)S(1)} %bitcast.45), channel_id=1, source_target_pairs={{0,1},{1,0},{2,3},{3,2},{4,5},{5,4},{6,7},{7,6},{8,9},{9,8},{10,11... | collective-permute-start | bytes 12582920 | tf_op jit(solution)/shard_map/ppermute | solution.py:287
  225.2 49.5 %copy-start = (f32[256,2048]{1,0:T(8,128)S(1)}, f32[256,2048]{1,0:T(8,128)}, u32[]{:S(2)}) copy-start(f32[256,2048]{1,0:T(8,128)} %get-tuple-element.10) | copy-start | bytes 6291460
  225.5 47.7 %collective-permute-start.1 = (bf16[256,2048]{1,0:T(8,128)(2,1)S(1)}, bf16[256,2048]{1,0:T(8,128)(2,1)S(1)}, u32[]{:S(2)}, u32[]{:S(2)}) collective-permute-start(bf16[256,2048]{1,0:T(8,128)(2,1)S(1)} %get-tuple-element.17), channel_id=1, source_target_pairs={{0,2},{2,0},{8,10},{10,8},{1,3},{3,1},{9,11},{11,9},{4,6},{6,4},{1... | collective-permute-start | bytes 3145736 | tf_op jit(solution)/shard_map/ppermute | solution.py:291
  227.1 46.1 %collective-permute-start.3 = (bf16[256,2048]{1,0:T(8,128)(2,1)S(1)}, bf16[256,2048]{1,0:T(8,128)(2,1)S(1)}, u32[]{:S(2)}, u32[]{:S(2)}) collective-permute-start(bf16[256,2048]{1,0:T(8,128)(2,1)S(1)} %get-tuple-element.18), channel_id=1, source_target_pairs={{0,10},{2,8},{8,2},{10,0},{1,11},{3,9},{9,3},{11,1},{4,14},{6,12},... | collective-permute-start | bytes 3145736 | tf_op jit(solution)/shard_map/ppermute | solution.py:291
  228.5 46.2 %collective-permute-start.2 = (bf16[256,2048]{1,0:T(8,128)(2,1)S(1)}, bf16[256,2048]{1,0:T(8,128)(2,1)S(1)}, u32[]{:S(2)}, u32[]{:S(2)}) collective-permute-start(bf16[256,2048]{1,0:T(8,128)(2,1)S(1)} %get-tuple-element.19), channel_id=1, source_target_pairs={{0,8},{2,10},{8,0},{10,2},{1,9},{3,11},{9,1},{11,3},{4,12},{6,14},... | collective-permute-start | bytes 3145736 | tf_op jit(solution)/shard_map/ppermute | solution.py:291

commit v2 on v1

--- a/solution.py
+++ b/solution.py
@@ -59,8 +59,11 @@
     return jnp.where(keep, full, 0.0).astype(BF16)
 
 
-def front(sizes, x_ref, b_ref, c_ref, a_ref, k_ref, wo_ref, res_ref, gain_ref, *rest):
+def layer(sizes, fused, x_ref, b_ref, c_ref, a_ref, k_ref, wo_ref, res_ref, gain_ref, *rest):
     quarters, rest = rest[:3], rest[3:]
+    if fused:
+        out_ref, *rest = rest
+        hidden, partners, peers, *rest = rest
     weights, (rows_ref, carried_ref), rest = rest[:3], rest[3:5], rest[5:]
     (work, read_in, read_out, ends, total, gathered, act, share, others,
      send_sem, recv_sem, local_sem) = rest
@@ -274,13 +277,99 @@
                     last.append(send(
                         rows_ref.at[0, k], rows_ref.at[t, k], (h, u, m, v, lax.rem(core + t, tp))
                     ))
-    for copy in (*over_m.values(), *last):
+    sent = [*first.values(), *over_h.values(), *over_m.values(), *states_out, *mixed_copies]
+    row_sends = [*row_copies.values(), *last]
+    for (w, *_), copy in over_m.items():
+        if w < 2 or not fused:
+            copy.wait_recv()
+    for copy in last:
         copy.wait_recv()
-    for copy in (*first.values(), *over_h.values(), *over_m.values(), *states_out,
-                 *mixed_copies, *row_copies.values(), *last):
-        copy.wait_send()
     for copy in locals_:
         copy.wait()
+    if fused:
+        sent += back(
+            sizes, send, peer, (h, u, m, v, core), weights, rows_ref, carried_ref, out_ref,
+            hidden, partners, peers, row_sends, [c for (w, *_), c in over_m.items() if w == 2],
+        )
+    else:
+        sent += row_sends
+    for copy in sent:
+        copy.wait_send()
+
+
+def back(sizes, send, peer, here, weights, rows_ref, carried_ref, out_ref, hidden, partners,
+         peers, row_sends, down_copies):
+    tp = sizes["tp"]
+    h, u, m, v, core = here
+    _, _, keep_rows, width = rows_ref.shape
+    across = (((1,), (1,)), ((), ()))
+
+    @pl.loop(0, 4 * tp)
+    def _(i):
+        t, k = lax.div(i, 4), lax.rem(i, 4)
+        block = rows_ref[t, k]
+        gate = lax.dot_general(block, weights[0][...], across, preferred_element_type=F32)
+        up = lax.dot_general(block, weights[1][...], across, preferred_element_type=F32)
+        hidden[i] = (jax.nn.silu(gate) * up).astype(BF16)
+
+    for copy in (*down_copies,):
+        copy.wait_recv()
+    for copy in row_sends:
+        copy.wait_send()
+
+    tile = min(512, width)
+    line = min(32, keep_rows)
+    sent = []
+    peer_copies = []
+    from_core = {}
+
+    def reduce(k):
+        for copy in from_core[k]:
+            copy.wait_recv()
+
+        @pl.loop(0, keep_rows // line)
+        def _(i):
+            at = pl.ds(pl.multiple_of(i * line, line), line)
+            total = rows_ref[0, k, at, :].astype(F32)
+            for t in range(1, tp):
+                total = total + partners[k, t - 1, at, :].astype(F32)
+            rows_ref[0, k, at, :] = total.astype(BF16)
+
+        if k:
+            pu, pv = peer(k)
+            peer_copies.append(send(rows_ref.at[0, k], peers.at[k - 1], (h, pu, m, pv, core)))
+
+    order = (3, 1, 2, 0)
+    for step, k in enumerate(order):
+        from_core[k] = []
+        for t in (*range(1, tp), 0):
+            @pl.loop(0, width // tile)
+            def _(j):
+                at = pl.ds(pl.multiple_of(j * tile, tile), tile)
+                rows_ref[t, k, :, at] = jnp.dot(
+                    hidden[t * 4 + k], weights[2][:, at], preferred_element_type=F32
+                ).astype(BF16)
+
+            if t:
+                from_core[k].append(send(
+                    rows_ref.at[t, k], partners.at[k, t - 1],
+                    (h, u, m, v, lax.rem(core + tp - t, tp)),
+                ))
+        reduce(k)
+        sent += from_core[k]
+    for copy in peer_copies:
+        copy.wait_recv()
+
+    @pl.loop(0, keep_rows // line)
+    def _(i):
+        at = pl.ds(pl.multiple_of(i * line, line), line)
+        total = rows_ref[0, 0, at, :].astype(F32)
+        for k in range(1, 4):
+            total = total + peers[k - 1, at, :].astype(F32)
+        total = total.astype(BF16).astype(F32)
+        out_ref[at, :] = (carried_ref[at, :] + 0.5 * total).astype(BF16)
+
+    return sent + peer_copies
 
 
 def shift(value, axis, count, by):
@@ -316,15 +405,29 @@
     copies = 3 * (3 + 4 * (nh - 1) + 4 * nh * (nm - 1)) + (n - 1) + (tp - 1) + 3 + 4 * (tp - 1)
     laid = (part, n * depth) if depth % 128 == 0 else (n, part, depth)
     vmem = pl.BlockSpec(memory_space=pltpu.VMEM)
-    full_gate, full_up, full_down, rows_all, carried = pl.pallas_call(
-        functools.partial(front, sizes),
+    between = [(laid, BF16)] * 3 + [
+        ((tp, 4, keep_rows, width), BF16), ((keep_rows, width), F32),
+    ]
+    fused = depth % 128 == 0
+    if fused:
+        copies += 4 * (tp - 1) + 3
+        out_shape = [jax.ShapeDtypeStruct((keep_rows, width), BF16)]
+        extra = [
+            pltpu.VMEM((4 * tp, keep_rows, part), BF16),
+            pltpu.VMEM((4, tp - 1, keep_rows, width), BF16),
+            pltpu.VMEM((3, keep_rows, width), BF16),
+            *(pltpu.VMEM(*item) for item in between),
+        ]
+    else:
+        out_shape = [jax.ShapeDtypeStruct(*item) for item in between]
+        extra = []
+    results = pl.pallas_call(
+        functools.partial(layer, sizes, fused),
         in_specs=[vmem] * 11,
-        out_specs=[vmem] * 5,
-        out_shape=[jax.ShapeDtypeStruct(laid, BF16)] * 3 + [
-            jax.ShapeDtypeStruct((tp, 4, keep_rows, width), BF16),
-            jax.ShapeDtypeStruct((keep_rows, width), F32),
-        ],
+        out_specs=[vmem] * len(out_shape),
+        out_shape=out_shape,
         scratch_shapes=[
+            *extra,
             pltpu.VMEM((rows, 2 * sb), F32),
             pltpu.VMEM((blocks, cb, 2 * sb), BF16),
             pltpu.VMEM((blocks, 2 * sb, cb), BF16),
@@ -339,12 +442,15 @@
             pltpu.SemaphoreType.DMA((3,)),
         ],
         compiler_params=pltpu.CompilerParams(
-            collective_id=0, has_side_effects=True, vmem_limit_bytes=60 * 2**20
+            collective_id=0, has_side_effects=True, vmem_limit_bytes=62 * 2**20
         ),
-        name="front",
+        name="layer",
     )(x, read_in, read_out, power, skip.reshape(blocks, 1, cb), out_proj, residual,
       norm_gain.reshape(1, width), w_gate.T.reshape(4, part, depth),
       w_up.T.reshape(4, part, depth), w_down.reshape(4, part, depth))
+    if fused:
+        return results[0]
+    full_gate, full_up, full_down, rows_all, carried = results
     if len(laid) == 3:
         full_gate, full_up, full_down = (
             t.transpose(1, 0, 2).reshape(part, width) for t in (full_gate, full_up, full_down)

time: 277 us -> 229 us (0.83)
  waiting for transfers between devices: 52.7 us -> 0 us
  Pallas kernels: 166 us -> 214 us
  matrix products: 30.3 us -> 0 us
  other arithmetic: 11.6 us -> 6.54 us
  local copies, waits for them, and re-layouts: 11.8 us -> 7.27 us
  starting transfers between devices: 3.62 us -> 0 us
    ppermute x4 -> x0, waiting for transfers between devices: 52.7 us -> none  [the longest x3 45.6 us: flip(): return lax.ppermute(value, axes, [(i, i ^ k) for i in range(count)])]
    pallas_call x1, Pallas kernels: 166 us -> 214 us  [on_device(): pl.pallas_call(functools.partial(layer, sizes, fused), in_specs=[vmem] *...]
    dot_general x2 -> x0, matrix products: 30.3 us -> none  [the longest x1 19.1 us: on_device(): down = jnp.dot(hidden, full_down, preferred_element_type=F32).astype(BF16)]
    slice x1 -> x0, local copies, waits for them, and re-layouts: 4.11 us -> none  [on_device(): summed = summed + shift(down[t], 'tp', tp, -t).astype(F32)]
    convert_element_type x2 -> x0, other arithmetic: 4.09 us -> none  [the longest x1 2.29 us: on_device(): summed = summed.astype(BF16)]
    ppermute x4 -> x0, starting transfers between devices: 3.62 us -> none  [the longest x3 3.55 us: flip(): return lax.ppermute(value, axes, [(i, i ^ k) for i in range(count)])]
  transfers between devices with their start and end apart: 4 -> 0, of which waited for: 3 -> 0; matrix products, arithmetic and copies ran while one was open for 0% -> 0% of each run, Pallas kernels for 0% -> 0%
where the time goes in v2:
time: 229 us; the launch traced here: 228 us
  Pallas kernels  214 us (93%)
  local copies, waits for them, and re-layouts  7.27 us (3%)
  other arithmetic  6.54 us (3%)
    pallas_call x1, Pallas kernels, on_device(): pl.pallas_call(functools.partial(layer, sizes, fused), in_specs=[vmem] *...  214 us

profile of v2, /device:TPU:0, one launch (start us, length us, event | category | flops | bytes accessed | tf_op | source)
XLA Modules:
  0.0 228.3 jit_solution(12036325246399897482)
XLA Ops:
  0.0 0.7 exp.6
  0.7 0.9 cosine_multiply_fusion
  1.6 0.1 stack_reshape.21
  1.6 0.1 stack_reshape.22
  1.7 0.6 pad_maximum_fusion.2.a_ref
  2.3 1.0 convert_bitcast_fusion
  3.3 1.0 fusion
  4.3 1.1 subtract_convert_fusion
  5.4 0.0 copy-start.2
  5.4 0.8 pad_maximum_fusion.1.b_ref
  6.2 0.3 copy.41
  6.5 0.3 copy.40
  6.8 0.0 copy-start
  6.8 1.2 pad_maximum_fusion.c_ref
  8.0 0.0 copy-done.2
  8.0 0.0 copy-start.1
  8.0 0.1 reshape.37
  8.1 1.1 copy.45
  9.2 0.0 copy-done
  9.2 1.2 copy.38
  10.4 0.0 copy-done.1
  10.4 1.1 copy.39
  11.5 214.5 %layer.1 = bf16[256,2048]{1,0:T(8,128)(2,1)} custom-call(bf16[4,512,128]{2,1,0:T(8,128)(2,1)} %bitcast.28, bf16[4,2,128,64]{3,2,1,0:T(8,128)(2,1)} %pad_maximum_fusion.1.b_ref, bf16[4,2,512,16]{3,2,1,0:T(8,128)(2,1)} %pad_maximum_fusion.c_ref, f32[4,2,512]{2,1,0:T(2,128)} %pad_maximum_fusion.2.a_ref, f32[4,1,128]{2,1,0:T(1,128)} %bitcast.35, ...), custom_call_target="tpu_custom_call" | custom-call | tf_op jit(solution)/shard_map/layer/pallas_call | solution.py:424
  226.0 2.3 %copy.47 = bf16[256,2048]{1,0:T(8,128)(2,1)} copy(bf16[256,2048]{1,0:T(8,128)(2,1)} %layer.1) | data formatting | bytes 2097152
Async XLA Ops:
  5.4 2.6 %copy-start.2 = (bf16[512,512]{1,0:T(8,128)(2,1)S(1)}, bf16[512,512]{1,0:T(8,128)(2,1)}, u32[]{:S(2)}) copy-start(bf16[512,512]{1,0:T(8,128)(2,1)} %param.15) | copy-start | bytes 1572868
  6.8 2.5 %copy-start = (bf16[128,2816]{1,0:T(8,128)(2,1)S(1)}, bf16[128,2816]{1,0:T(8,128)(2,1)}, u32[]{:S(2)}) copy-start(bf16[128,2816]{1,0:T(8,128)(2,1)} %param.27) | copy-start | bytes 2162692
  8.0 2.5 %copy-start.1 = (bf16[128,2816]{1,0:T(8,128)(2,1)S(1)}, bf16[128,2816]{1,0:T(8,128)(2,1)}, u32[]{:S(2)}) copy-start(bf16[128,2816]{1,0:T(8,128)(2,1)} %param.28) | copy-start | bytes 2162692
